TPU v7x, 32 devices: a whole 2x2x4 slice. The times are simulated.
32 devices in a mesh: ep: 8 (over z, y), tp: 4 (over x, core).
Axes of the slice: x: 2, y: 2, z: 4, core: 2. Of those that a mesh axis runs over, the one named last changes fastest.
Arguments:
- q_heads: bfloat16 [8192, 1024], P('ep', 'tp'), may hold values from -200 to 200
- k_heads: bfloat16 [8192, 256], P('ep', 'tp'), may hold values from -6 to 6
- v_heads: bfloat16 [8192, 256], P('ep', 'tp'), may hold values from -6 to 6
- sink_logits: float32 [16], P('tp'), may hold values from 1 to 5
- out_weight: bfloat16 [1024, 2048], P(None, 'tp'), may hold values from -1.5 to 1.5
- tokens_b: bfloat16 [4096, 2048], P('ep'), may hold values from -6 to 6
- moe_gain: float32 [2048], replicated, may hold values from 0.1 to 1.9
- router_group: bfloat16 [2048, 4], replicated, may hold values from -0.125 to 0.125
- router_expert: bfloat16 [2048, 16], replicated, may hold values from -0.125 to 0.125
- route_expert: int32 [4096, 2], P('ep'), may hold values from 0 to 15, as said below
- expert_gate: bfloat16 [16, 2048, 1024], P('ep', None, 'tp'), may hold values from -0.125 to 0.125
- expert_up: bfloat16 [16, 2048, 1024], P('ep', None, 'tp'), may hold values from -0.125 to 0.125
- expert_down: bfloat16 [16, 1024, 2048], P('ep', 'tp'), may hold values from -0.75 to 0.75
Outputs:
- mixer_out: bfloat16 [8192, 2048], P('ep', 'tp')
- moe_out: bfloat16 [4096, 2048], P(('ep', 'tp'))
Inputs may be any that keep to these rules, and one draw needn't show every extreme that they name: `route_expert`: each token names two different experts, in rising order, of one group of 4 consecutive experts. In each aligned block of 128 rows (the rows of one device) no expert is named by more than 32 tokens, in each group one expert is named by exactly 32 tokens of every block, and each group is named by a quarter of every block's tokens.
All inputs are finite; a program needn't handle non-finite values.
Results may differ from a plain program's by a relative error of at most 0.011.
Values may be sent and summed in bfloat16 or wider, within the bound.
A program may use at most 128 MiB of HBM per device.

v0:
```python
import jax
import jax.numpy as jnp
from jax import lax
from jax.sharding import PartitionSpec as P

HEADS = 16
KV = 4
HD = 64
WINDOW = 128


def shifted(value, axis, steps):
    count = lax.axis_size(axis)
    leading, last = (max(0, -steps), min(count, count - steps))
    return lax.ppermute(value, axis, [(source, source + steps) for source in range(leading, last)])


def normalize(rows_in, gain):
    values = rows_in.astype(jnp.float32)
    scaled = values * lax.rsqrt(jnp.mean(values * values, axis=-1, keepdims=True) + 1e-06) * gain
    return scaled.astype(jnp.bfloat16)


def gate_weights(normed, routes, router_group, router_expert):
    group_logits = jnp.dot(normed, router_group, preferred_element_type=jnp.float32)
    expert_logits = jnp.dot(normed, router_expert, preferred_element_type=jnp.float32)
    group_count = router_group.shape[1]
    expert_count = router_expert.shape[1]
    chosen_group = routes[:, 0] // (expert_count // group_count)
    group_match = chosen_group[:, None] == jnp.arange(group_count, dtype=jnp.int32)[None, :]
    group_share = jnp.sum(
        jnp.where(group_match, jax.nn.softmax(group_logits, axis=-1), 0.0), axis=-1
    )
    expert_match = routes[:, :, None] == jnp.arange(expert_count, dtype=jnp.int32)[None, None, :]
    picked = jnp.sum(jnp.where(expert_match, expert_logits[:, None, :], 0.0), axis=-1)
    return group_share[:, None] * jax.nn.softmax(picked, axis=-1)


def slot_positions(routes, sub_count, expert_count):
    flat_routes = routes.reshape(sub_count, -1)
    onehot = (
        flat_routes[:, :, None] == jnp.arange(expert_count, dtype=jnp.int32)[None, None, :]
    ).astype(jnp.int32)
    places = jnp.sum(onehot * jnp.cumsum(onehot, axis=1), axis=2) - 1
    return (flat_routes, places)


def fill_slots(normed, flat_routes, places, sub_count, expert_count, capacity, exp_local):
    sub_index = jnp.arange(sub_count, dtype=jnp.int32)[:, None]
    target = ((flat_routes * sub_count + sub_index) * capacity + places).reshape(-1)
    source = jnp.repeat(normed, 2, axis=0)
    buffer = jnp.zeros((expert_count * sub_count * capacity, normed.shape[1]), jnp.bfloat16)
    buffer = buffer.at[target].set(source)
    return buffer.reshape(
        expert_count // exp_local, exp_local, sub_count, capacity, normed.shape[1]
    )


def per_device(
    q_heads,
    k_heads,
    v_heads,
    sink_logits,
    out_weight,
    tokens_b,
    moe_gain,
    router_group,
    router_expert,
    route_expert,
    expert_gate,
    expert_up,
    expert_down,
):
    span_len = WINDOW
    row_count = q_heads.shape[0]
    kv_local = k_heads.shape[1] // HD
    group_size = HEADS // KV
    blocks = row_count // span_len
    stacked = jnp.stack([k_heads[row_count - span_len :], v_heads[row_count - span_len :]])
    earlier = shifted(stacked, "ep", 1)

    def make_band(own_rows, prev_rows):
        extended = jnp.concatenate([prev_rows, own_rows], axis=0).reshape(
            blocks + 1, span_len, kv_local, HD
        )
        return jnp.concatenate([extended[:-1], extended[1:]], axis=1)

    key_band = make_band(k_heads, earlier[0])
    value_band = make_band(v_heads, earlier[1])
    query_blocks = q_heads.reshape(blocks, span_len, kv_local, group_size, HD)
    scores = jnp.einsum(
        "nqhgd,nkhd->nhgqk", query_blocks, key_band, preferred_element_type=jnp.float32
    ) * HD ** (-0.5)
    first_row = lax.axis_index("ep") * row_count
    query_index = jnp.arange(span_len, dtype=jnp.int32)[:, None]
    key_index = jnp.arange(2 * span_len, dtype=jnp.int32)[None, :]
    distance = query_index + span_len - key_index
    key_place = (
        first_row
        + jnp.arange(blocks, dtype=jnp.int32)[:, None, None] * span_len
        + key_index[None]
        - span_len
    )
    allowed = (distance >= 0)[None] & (distance < span_len)[None] & (key_place >= 0)
    masked = jnp.where(allowed[:, None, None], scores, -1e30)
    sink_full = sink_logits.reshape(kv_local, group_size)[None, :, :, None]
    row_max = jnp.maximum(jnp.max(masked, axis=-1), sink_full)
    weights_exp = jnp.exp(masked - row_max[..., None])
    denominator = jnp.sum(weights_exp, axis=-1) + jnp.exp(sink_full - row_max)
    probs = (weights_exp / denominator[..., None]).astype(jnp.bfloat16)
    attended = jnp.einsum(
        "nhgqk,nkhd->nqhgd", probs, value_band, preferred_element_type=jnp.float32
    )
    attended = attended.astype(jnp.bfloat16).reshape(row_count, kv_local * group_size * HD)
    mixed = jnp.dot(
        lax.all_gather(attended, "tp", axis=1, tiled=True),
        out_weight,
        preferred_element_type=jnp.float32,
    )
    mixer_out = mixed.astype(jnp.bfloat16)
    tp_count = lax.axis_size("tp")
    tp_index = lax.axis_index("tp")
    exp_local = expert_gate.shape[0]
    expert_count = exp_local * lax.axis_size("ep")
    rows_dev = tokens_b.shape[0] // tp_count
    capacity = min(4 * rows_dev // expert_count, rows_dev // 4)
    own_routes = lax.dynamic_slice_in_dim(route_expert, tp_index * rows_dev, rows_dev, 0)
    own_normed = normalize(
        lax.dynamic_slice_in_dim(tokens_b, tp_index * rows_dev, rows_dev, 0), moe_gain
    )
    flat_routes, places = slot_positions(own_routes, 1, expert_count)
    buffer = fill_slots(own_normed, flat_routes, places, 1, expert_count, capacity, exp_local)
    delivered = lax.all_to_all(buffer, "ep", split_axis=0, concat_axis=0, tiled=True)
    arrived = lax.all_gather(delivered, "tp", axis=2, tiled=True)
    own_flat = flat_routes[0]
    own_places = places[0]
    gates = gate_weights(own_normed, own_routes, router_group, router_expert)
    gate_pre = jnp.einsum(
        "setcd,edf->setcf", arrived, expert_gate, preferred_element_type=jnp.float32
    )
    up_pre = jnp.einsum("setcd,edf->setcf", arrived, expert_up, preferred_element_type=jnp.float32)
    activated = (jax.nn.silu(gate_pre) * up_pre).astype(jnp.bfloat16)
    partial_value = jnp.einsum(
        "setcf,efd->setcd", activated, expert_down, preferred_element_type=jnp.float32
    )
    summed = lax.psum_scatter(
        partial_value.astype(jnp.bfloat16), "tp", scatter_dimension=2, tiled=True
    )
    returned = lax.all_to_all(summed, "ep", split_axis=0, concat_axis=0, tiled=True)
    returned = returned.reshape(expert_count * capacity, returned.shape[-1])
    picked_rows = returned[own_flat * capacity + own_places].reshape(
        rows_dev, 2, returned.shape[-1]
    )
    moe_out = jnp.sum(gates[:, :, None] * picked_rows.astype(jnp.float32), axis=1).astype(
        jnp.bfloat16
    )
    return (mixer_out, moe_out)


def solution(mesh):
    in_specs = (
        P("ep", "tp"),
        P("ep", "tp"),
        P("ep", "tp"),
        P("tp"),
        P(None, "tp"),
        P("ep", None),
        P(),
        P(),
        P(),
        P("ep", None),
        P("ep", None, "tp"),
        P("ep", None, "tp"),
        P("ep", "tp", None),
    )
    out_specs = (P("ep", "tp"), P(("ep", "tp"), None))
    return jax.shard_map(
        per_device, mesh=mesh, in_specs=in_specs, out_specs=out_specs, check_vma=False
    )
```

profile of v0, /device:TPU:0, one launch (start us, length us, event | category | flops | bytes accessed | tf_op | source)
XLA Modules:
  0.0 384.7 jit_solution(17518008943013169215)
XLA Ops:
  7.2 0.8 broadcast_multiply_fusion
  8.3 0.6 reduce-window.6
  9.7 1.2 fusion.24
  10.9 1.3 fusion.26
  12.2 1.6 broadcast_in_dim.34
  13.8 2.3 reshape.383
  16.0 4.4 %scatter_custom_fusion = bf16[512,2048]{1,0:T(8,128)(2,1)} fusion(s32[256]{0:T(256)S(1)} %bitcast.171, bf16[256,2048]{1,0:T(8,128)(2,1)} %reshape.383, bf16[]{:T(256)} %constant.67.clone.1), kind=kCustom, calls=%fused_computation.35 | custom fusion | bytes 2097664 | tf_op jit(solution)/shard_map/scatter | solution.py:53
  20.5 55.5 %all_to_all.10 = bf16[8,2,1,32,2048]{4,3,2,1,0:T(8,128)(2,1)S(1)} all-to-all(bf16[8,2,1,32,2048]{4,3,2,1,0:T(8,128)(2,1)} %bitcast.159), channel_id=1, replica_groups=mesh['ep'=8,'tp'=4] {'ep'}, dimensions={0} | all-to-all | bytes 4194304 | tf_op jit(solution)/shard_map/all_to_all | solution.py:133
  76.0 1.5 copy.69
  77.6 57.4 %all-gather.5.cloned.1.call-done = bf16[8,2,4,32,2048]{4,3,2,0,1:T(8,128)(2,1)} async-done(((bf16[8,2,1,32,2048]{4,3,2,0,1:T(8,128)(2,1)}), bf16[8,2,4,32,2048]{4,3,2,0,1:T(8,128)(2,1)}) %all-gather.5.cloned.1.call-update) | async-done | bytes 8388624 | tf_op jit(solution)/shard_map/all_gather | solution.py:134
  134.9 7.7 %fusion.3 = f32[2,8,4,32,256]{4,3,2,1,0:T(8,128)} fusion(bf16[8,2,4,32,2048]{4,3,2,0,1:T(8,128)(2,1)} %all-gather.5.cloned.1.call-done, bf16[2,2048,256]{2,1,0:T(8,128)(2,1)} %param.24), kind=kOutput, calls=%fused_computation.9 | convolution fusion | flops 2147483648 | bytes 12582912 | tf_op jit(solution)/shard_map/setcd,edf->setcf/dot_general | solution.py:141
  142.6 13.5 %convert_bitcast_fusion = bf16[8,2,4,32,2048]{4,3,2,0,1:T(8,128)(2,1)} fusion(bf16[2,256,2048]{2,1,0:T(8,128)(2,1)S(1)} %copy-done, f32[2,8,4,32,256]{4,3,2,1,0:T(8,128)} %fusion.3, bf16[8,2,4,32,2048]{4,3,2,0,1:T(8,128)(2,1)} %all-gather.5.cloned.1.call-done, bf16[2,2048,256]{2,1,0:T(8,128)(2,1)} %param.23), kind=kOutput, calls=%fused_computation.2 | convolution fusion | flops 4302307328 | bytes 23068672 | tf_op jit(solution)/shard_map/setcf,efd->setcd/dot_general | solution.py:143
  156.1 0.9 copy-done.3
  157.1 3.6 collective-permute-start
  161.2 0.4 reshape.392
  161.7 0.6 dynamic-slice
  162.5 0.9 fusion.1
  163.5 1.1 fusion
  164.5 0.8 copy-done.2
  165.4 143.8 %all-reduce.3.cloned.1.call-done = bf16[8,2,4,32,2048]{4,3,2,0,1:T(8,128)(2,1)} async-done(((bf16[8,2,4,32,2048]{4,3,2,0,1:T(8,128)(2,1)}), bf16[8,2,4,32,2048]{4,3,2,0,1:T(8,128)(2,1)}) %all-reduce.3.cloned.1.call-update) | async-done | bytes 8388624
  309.2 2.5 constant_dynamic-slice_fusion
  311.6 1.6 copy.70
  313.2 5.5 %all-to-all-start.1 = ((bf16[8,2,1,32,2048]{4,3,2,1,0:T(8,128)(2,1)}), bf16[8,2,1,32,2048]{4,3,2,1,0:T(8,128)(2,1)S(1)}, u32[]{:S(2)}, u32[]{:S(2)}) async-start(bf16[8,2,1,32,2048]{4,3,2,1,0:T(8,128)(2,1)} %copy.70), calls=%async_computation.1 | async-start | bytes 4194304 | tf_op jit(solution)/shard_map/all_to_all | solution.py:149
  318.8 3.4 fusion.21
  322.2 0.3 copy.61
  322.6 0.9 copy.91
  324.3 22.5 %all-gather.3.cloned.1.call-done = bf16[1024,1024]{0,1:T(8,128)(2,1)} async-done(((bf16[1024,256]{0,1:T(8,128)(2,1)}), bf16[1024,1024]{0,1:T(8,128)(2,1)}) %all-gather.3.cloned.1.call-update) | async-done | bytes 2097168 | tf_op jit(solution)/shard_map/all_gather | solution.py:116
  346.8 4.1 %convolution_convert_fusion = bf16[1024,512]{1,0:T(8,128)(2,1)} fusion(bf16[1024,1024]{0,1:T(8,128)(2,1)} %all-gather.3.cloned.1.call-done, bf16[1024,512]{1,0:T(8,128)(2,1)} %param.17), kind=kOutput, calls=%fused_computation.24 | convolution fusion | flops 1074266112 | bytes 4194304 | tf_op jit(solution)/shard_map/dot_general | solution.py:115
  350.9 15.8 %all-to-all-done.1 = bf16[8,2,1,32,2048]{4,3,2,1,0:T(8,128)(2,1)S(1)} async-done(((bf16[8,2,1,32,2048]{4,3,2,1,0:T(8,128)(2,1)}), bf16[8,2,1,32,2048]{4,3,2,1,0:T(8,128)(2,1)S(1)}, u32[]{:S(2)}, u32[]{:S(2)}) %all-to-all-start.1) | async-done | bytes 2097184 | tf_op jit(solution)/shard_map/all_to_all | solution.py:149
  366.7 2.3 gather_fusion
  369.0 3.5 reshape.370
  372.6 5.6 %multiply_reduce_fusion = bf16[128,2048]{1,0:T(8,128)(2,1)} fusion(f32[128,2,2048]{2,1,0:T(2,128)} %reshape.370, f32[128,2]{1,0:T(8,128)S(1)} %copy.62), kind=kLoop, calls=%fused_computation.22 | loop fusion | flops 786432 | bytes 2622464 | tf_op jit(solution)/shard_map/reduce_sum | solution.py:154
  (72 shorter events, 2.9 us)
Async XLA Ops:
  7.2 135.4 %copy-start = (bf16[2,256,2048]{2,1,0:T(8,128)(2,1)S(1)}, bf16[2,256,2048]{2,1,0:T(8,128)(2,1)}, u32[]{:S(2)}) copy-start(bf16[2,256,2048]{2,1,0:T(8,128)(2,1)} %param.25) | copy-start | bytes 6291460
  7.2 127.8 %all-gather.5.cloned.1.call-start = ((), (), s32[]{:S(2)}) async-start(), calls=%async_computation.3 | async-start | bytes 10485760 | tf_op jit(solution)/shard_map/all_gather | solution.py:134
  77.5 231.6 %all-reduce.3.cloned.1.call-start = ((), (), s32[]{:S(2)}) async-start(), calls=%async_computation.4 | async-start | bytes 16777216
  156.1 0.9 copy-start.3
  156.1 1.0 copy-start.4
  156.1 5.1 %copy-start.5 = (bf16[1024,256]{1,0:T(8,128)(2,1)S(1)}, bf16[1024,256]{1,0:T(8,128)(2,1)}, u32[]{:S(2)}) copy-start(bf16[1024,256]{1,0:T(8,128)(2,1)} %param.13) | copy-start | bytes 1572868
  157.1 4.6 %copy-start.9 = (u32[32]{0:T(128)S(1)}, u32[32]{0:T(128)}, u32[]{:S(2)}) copy-start(u32[32]{0:T(128)} %constant.75) | copy-start | bytes 388
  157.1 5.2 %collective-permute-start = (bf16[2,128,64]{1,2,0:T(8,128)(2,1)S(1)}, bf16[2,128,64]{1,2,0:T(8,128)(2,1)S(1)}, u32[]{:S(2)}, u32[]{:S(2)}) collective-permute-start(bf16[2,128,64]{1,2,0:T(8,128)(2,1)S(1)} %pad_maximum_fusion.2), channel_id=1, source_target_pairs={{0,4},{4,8},{8,12},{12,16},{16,20},{20,24},{24,28},{1,5},{5,9},{9,... | collective-permute-start | bytes 98312 | tf_op jit(solution)/shard_map/ppermute | solution.py:15
  162.5 0.9 copy-start.8
  163.4 1.9 copy-start.2
  313.2 53.4 %all-to-all-start.1 = ((bf16[8,2,1,32,2048]{4,3,2,1,0:T(8,128)(2,1)}), bf16[8,2,1,32,2048]{4,3,2,1,0:T(8,128)(2,1)S(1)}, u32[]{:S(2)}, u32[]{:S(2)}) async-start(bf16[8,2,1,32,2048]{4,3,2,1,0:T(8,128)(2,1)} %copy.70), calls=%async_computation.1 | async-start | bytes 4194304 | tf_op jit(solution)/shard_map/all_to_all | solution.py:149
  318.8 28.0 %all-gather.3.cloned.1.call-start = ((), (), s32[]{:S(2)}) async-start(), calls=%async_computation.2 | async-start | bytes 2621440 | tf_op jit(solution)/shard_map/all_gather | solution.py:116
  322.2 1.3 copy-start.6
  322.2 1.6 copy-start.7
  369.0 9.1 %copy-start.1 = (bf16[2,256,2048]{2,1,0:T(8,128)(2,1)S(1)}, bf16[2,256,2048]{2,1,0:T(8,128)(2,1)}, u32[]{:S(2)}) copy-start(bf16[2,256,2048]{2,1,0:T(8,128)(2,1)} %param.25) | copy-start | bytes 6291460
Sparse Core Ops, SparseCore 0:
  77.6 57.2 all-gather.4
  156.3 152.8 all-reduce.2
  323.6 23.1 all-gather.2
where the time goes:
time: 385 us
  waiting for transfers between devices  239 us (62%)
  blocking collectives  55.5 us (14%)
  matrix products  30.1 us (8%)
  local copies, waits for them, and re-layouts  24.9 us (6%)
  between operations  14.1 us (4%)
  other arithmetic  11.5 us (3%)
  starting transfers between devices  9.2 us (2%)
    unnamed x4, waiting for transfers between devices  144 us
    all_gather x1, waiting for transfers between devices, per_device(): arrived = lax.all_gather(delivered, 'tp', axis=2, tiled=True)  57.4 us
    all_to_all x1, blocking collectives, per_device(): lax.all_to_all(buffer, 'ep', split_axis=0, concat_axis=0, tiled=True)  55.5 us
    all_gather x1, waiting for transfers between devices, per_device(): lax.all_gather(attended, 'tp', axis=1, tiled=True)  22.5 us
    all_to_all x1, waiting for transfers between devices, per_device(): lax.all_to_all(summed, 'ep', split_axis=0, concat_axis=0, tiled=True)  15.8 us
    dot_general x1, matrix products, per_device(): jnp.einsum('setcf,efd->setcd', activated, expert_down, preferred_element_...  13.5 us
  transfers between devices with their start and end apart: 5, of which 4 were waited for; matrix products, arithmetic and copies ran while one was open for 3% of the time, Pallas kernels for 0%

commit v1 on v0

--- a/solution.py
+++ b/solution.py
@@ -1,6 +1,10 @@
+import functools
+
 import jax
 import jax.numpy as jnp
 from jax import lax
+from jax.experimental import pallas as pl
+from jax.experimental.pallas import tpu as pltpu
 from jax.sharding import PartitionSpec as P
 
 HEADS = 16
@@ -54,6 +58,293 @@
     return buffer.reshape(
         expert_count // exp_local, exp_local, sub_count, capacity, normed.shape[1]
     )
+
+
+LANES = 128
+MESH = pl.DeviceIdType.MESH
+
+
+def moe_kernel(
+    groups,
+    xs_ref,
+    gate_hbm,
+    up_hbm,
+    down_hbm,
+    out_ref,
+    rows,
+    part,
+    wg,
+    wu,
+    wd,
+    act,
+    from_core,
+    relay_x,
+    relay_y,
+    from_x,
+    from_y,
+    total,
+    back,
+    load_sem,
+    send_sem,
+    recv_sem,
+):
+    ep, tp = lax.axis_index("ep"), lax.axis_index("tp")
+    group, member = ep // 2, ep % 2
+    x, core = tp // 2, tp % 2
+    tp_x, tp_c = (1 - x) * 2 + core, x * 2 + (1 - core)
+    ep_y = group * 2 + (1 - member)
+    x_dev, y_dev, c_dev = (ep, tp_x), (ep_y, tp), (ep, tp_c)
+    width = xs_ref.shape[1]
+    block = xs_ref.shape[0]
+    depth = out_ref.shape[1]
+    chunk = block // groups
+    half = block // 2
+    hidden = wg.shape[2]
+    lo, hi = pl.ds(0, half), pl.ds(half, half)
+    own = member * 4 + tp
+    slot_x = member * 4 + tp_x
+    slot_y = (1 - member) * 4 + tp
+    slot_d = (1 - member) * 4 + tp_x
+    mate = 1 - 2 * core
+
+    loads = [
+        pltpu.make_async_copy(source, held, load_sem.at[i])
+        for i, (source, held) in enumerate(((gate_hbm, wg), (up_hbm, wu), (down_hbm, wd)))
+    ]
+    for load in loads:
+        load.start()
+
+    planes = [((group + step) % groups) for step in range(1, groups)]
+    barrier = pltpu.get_barrier_semaphore()
+    peers = [(plane * 2 + member, tp) for plane in planes] + [x_dev, y_dev, c_dev]
+    for peer in peers:
+        pl.semaphore_signal(barrier, inc=1, device_id=peer, device_id_type=MESH)
+    pl.semaphore_wait(barrier, len(peers))
+
+    started = []
+
+    def send(index, source, target, device):
+        copy = pltpu.make_async_remote_copy(
+            src_ref=source,
+            dst_ref=target,
+            send_sem=send_sem.at[index],
+            recv_sem=recv_sem.at[index],
+            device_id=device,
+            device_id_type=MESH,
+        )
+        copy.start()
+        started.append(copy)
+        return copy
+
+    my_chunk = pl.ds(pl.multiple_of(group * chunk, chunk), chunk)
+    keep = pltpu.make_async_copy(xs_ref.at[my_chunk], rows.at[own, my_chunk], load_sem.at[3])
+    keep.start()
+    z_out = []
+    for step, plane in enumerate(planes):
+        there = pl.ds(pl.multiple_of(plane * chunk, chunk), chunk)
+        z_out.append(
+            send(step, xs_ref.at[there], rows.at[own, my_chunk], (plane * 2 + member, tp))
+        )
+    keep.wait()
+    for copy in z_out:
+        copy.wait_recv()
+
+    base = groups - 1
+    own_c = send(base, rows.at[own], rows.at[own], c_dev)
+    x_lo = send(base + 1, rows.at[own, lo], rows.at[own, lo], x_dev)
+    y_hi = send(base + 2, rows.at[own, hi], rows.at[own, hi], y_dev)
+    x_hi = send(base + 3, rows.at[own, hi], rows.at[own, hi], x_dev)
+    y_lo = send(base + 4, rows.at[own, lo], rows.at[own, lo], y_dev)
+    for load in loads:
+        load.wait()
+
+    def experts(slot):
+        first = slot - core
+        batch = 2 * block
+        pair = pl.ds(first, 2)
+
+        tokens = rows[pair, :, :depth].reshape(batch, depth)
+        shares = rows[pair, :, depth:].reshape(batch, LANES).astype(jnp.float32)
+        lane = lax.broadcasted_iota(jnp.int32, shares.shape, 1) % (LANES // 2)
+
+        def one(e, carry):
+            share = jnp.sum(
+                jnp.where(lane == member * wg.shape[0] + e, shares, 0.0), axis=1, keepdims=True
+            )
+            pre = jnp.dot(tokens, wg[e], preferred_element_type=jnp.float32)
+            up = jnp.dot(tokens, wu[e], preferred_element_type=jnp.float32)
+            act[e] = (jax.nn.silu(pre) * up * share).astype(jnp.bfloat16)
+            return carry
+
+        lax.fori_loop(0, wg.shape[0], one, 0)
+        acts = jnp.concatenate([act[e] for e in range(wg.shape[0])], axis=1)
+        tile = 512
+
+        def column(n, carry):
+            columns = pl.ds(pl.multiple_of(n * tile, tile), tile)
+            value = jnp.dot(acts, wd[:, columns], preferred_element_type=jnp.float32)
+            part[pair, :, columns] = value.astype(jnp.bfloat16).reshape(2, block, tile)
+            return carry
+
+        lax.fori_loop(0, depth // tile, column, 0)
+
+    own_c.wait_recv()
+    experts(own)
+    give = base + 5
+    sum_own = send(give, part.at[own + mate], from_core.at[0], c_dev)
+
+    x_lo.wait_recv()
+    relay_to_y = send(give + 1, rows.at[slot_x, lo], rows.at[slot_x, lo], y_dev)
+    y_hi.wait_recv()
+    relay_to_x = send(give + 2, rows.at[slot_y, hi], rows.at[slot_y, hi], x_dev)
+    x_hi.wait_recv()
+    x_core = send(give + 3, rows.at[slot_x], rows.at[slot_x], c_dev)
+    y_lo.wait_recv()
+    y_core = send(give + 4, rows.at[slot_y], rows.at[slot_y], c_dev)
+
+    x_core.wait_recv()
+    experts(slot_x)
+    sum_x = send(give + 5, part.at[slot_x + mate], from_core.at[1], c_dev)
+    y_core.wait_recv()
+    experts(slot_y)
+    sum_y = send(give + 6, part.at[slot_y + mate], from_core.at[2], c_dev)
+
+    relay_to_y.wait_recv()
+    relay_to_x.wait_recv()
+    d_core = send(give + 7, rows.at[slot_d], rows.at[slot_d], c_dev)
+
+    def add(target, index, other, other_index):
+        target[index] = (
+            target[index].astype(jnp.float32) + other[other_index].astype(jnp.float32)
+        ).astype(jnp.bfloat16)
+
+    sum_x.wait_recv()
+    add(part, slot_x, from_core, 1)
+    back_x_hi = send(give + 8, part.at[slot_x, hi], from_x.at[hi], x_dev)
+    sum_y.wait_recv()
+    add(part, slot_y, from_core, 2)
+    back_y_lo = send(give + 9, part.at[slot_y, lo], from_y.at[lo], y_dev)
+
+    d_core.wait_recv()
+    experts(slot_d)
+    sum_d = send(give + 10, part.at[slot_d + mate], from_core.at[3], c_dev)
+    sum_d.wait_recv()
+    add(part, slot_d, from_core, 3)
+    diag_y = send(give + 11, part.at[slot_d, lo], relay_y, y_dev)
+    diag_x = send(give + 12, part.at[slot_d, hi], relay_x, x_dev)
+    sum_own.wait_recv()
+    add(part, own, from_core, 0)
+    diag_y.wait_recv()
+    add(part, (slot_x, lo), relay_y, ...)
+    back_x_lo = send(give + 13, part.at[slot_x, lo], from_x.at[lo], x_dev)
+    diag_x.wait_recv()
+    add(part, (slot_y, hi), relay_x, ...)
+    back_y_hi = send(give + 14, part.at[slot_y, hi], from_y.at[hi], y_dev)
+    for copy in (back_x_hi, back_y_lo, back_x_lo, back_y_hi):
+        copy.wait_recv()
+    total[...] = (
+        part[own].astype(jnp.float32)
+        + from_x[...].astype(jnp.float32)
+        + from_y[...].astype(jnp.float32)
+    ).astype(jnp.bfloat16)
+
+    last = give + 15
+    home = []
+    for step, plane in enumerate(planes):
+        there = pl.ds(pl.multiple_of(plane * chunk, chunk), chunk)
+        home.append(
+            send(last + step, total.at[there], back.at[my_chunk], (plane * 2 + member, tp))
+        )
+    stay = pltpu.make_async_copy(total.at[my_chunk], back.at[my_chunk], load_sem.at[3])
+    stay.start()
+    stay.wait()
+    for copy in home:
+        copy.wait_recv()
+    out_ref[...] = back[...]
+    for copy in started:
+        copy.wait_send()
+
+
+def moe_exchange(sorted_rows, expert_gate, expert_up, expert_down, groups):
+    block, width = sorted_rows.shape
+    experts, depth, hidden = expert_gate.shape
+    down = expert_down.reshape(experts * hidden, depth)
+    copies = 2 * (groups - 1) + 20
+    bf16 = jnp.bfloat16
+    anywhere = pl.BlockSpec(memory_space=pl.ANY)
+    vmem = pl.BlockSpec(memory_space=pltpu.VMEM)
+    return pl.pallas_call(
+        functools.partial(moe_kernel, groups),
+        out_shape=jax.ShapeDtypeStruct((block, depth), bf16),
+        in_specs=[vmem, anywhere, anywhere, anywhere],
+        out_specs=vmem,
+        scratch_shapes=[
+            pltpu.VMEM((8, block, width), bf16),
+            pltpu.VMEM((8, block, depth), bf16),
+            pltpu.VMEM(expert_gate.shape, bf16),
+            pltpu.VMEM(expert_up.shape, bf16),
+            pltpu.VMEM(down.shape, bf16),
+            pltpu.VMEM((experts, 2 * block, hidden), bf16),
+            pltpu.VMEM((4, block, depth), bf16),
+            pltpu.VMEM((block // 2, depth), bf16),
+            pltpu.VMEM((block // 2, depth), bf16),
+            pltpu.VMEM((block, depth), bf16),
+            pltpu.VMEM((block, depth), bf16),
+            pltpu.VMEM((block, depth), bf16),
+            pltpu.VMEM((block, depth), bf16),
+            pltpu.SemaphoreType.DMA((4,)),
+            pltpu.SemaphoreType.DMA((copies,)),
+            pltpu.SemaphoreType.DMA((copies,)),
+        ],
+        cost_estimate=pl.CostEstimate(
+            flops=60_000_000_000, bytes_accessed=200_000_000, transcendentals=0
+        ),
+        compiler_params=pltpu.CompilerParams(
+            collective_id=0, has_side_effects=True, vmem_limit_bytes=48 * 2**20
+        ),
+    )(sorted_rows, expert_gate, expert_up, down)
+
+
+def moe_by_group(
+    tokens_b,
+    moe_gain,
+    router_group,
+    router_expert,
+    route_expert,
+    expert_gate,
+    expert_up,
+    expert_down,
+):
+    tp_count = lax.axis_size("tp")
+    tp_index = lax.axis_index("tp")
+    groups = router_group.shape[1]
+    group_experts = router_expert.shape[1] // groups
+    rows_dev = tokens_b.shape[0] // tp_count
+    routes = lax.dynamic_slice_in_dim(route_expert, tp_index * rows_dev, rows_dev, 0)
+    normed = normalize(
+        lax.dynamic_slice_in_dim(tokens_b, tp_index * rows_dev, rows_dev, 0), moe_gain
+    )
+    gates = gate_weights(normed, routes, router_group, router_expert)
+    lanes = jnp.arange(LANES // 2, dtype=jnp.int32)
+    share = jnp.sum(
+        jnp.where((routes % group_experts)[:, :, None] == lanes, gates[:, :, None], 0.0), axis=1
+    )
+    coarse = lax.reduce_precision(share, 8, 7)
+    extended = jnp.concatenate(
+        [normed, coarse.astype(jnp.bfloat16), (share - coarse).astype(jnp.bfloat16)], axis=1
+    )
+    named = routes[:, 0] // group_experts
+    same = named[:, None] == named[None, :]
+    order = jnp.arange(rows_dev, dtype=jnp.int32)
+    rank = jnp.sum((same & (order[None, :] < order[:, None])).astype(jnp.int32), axis=1)
+    place = named * (rows_dev // groups) + rank
+    take = (place[None, :] == order[:, None]).astype(jnp.bfloat16)
+    put = (place[:, None] == order[None, :]).astype(jnp.bfloat16)
+    sorted_rows = jnp.dot(take, extended, preferred_element_type=jnp.float32)
+    result = moe_exchange(
+        sorted_rows.astype(jnp.bfloat16), expert_gate, expert_up, expert_down, groups
+    )
+    return jnp.dot(put, result, preferred_element_type=jnp.float32).astype(jnp.bfloat16)
 
 
 def per_device(
@@ -118,6 +409,19 @@
         preferred_element_type=jnp.float32,
     )
     mixer_out = mixed.astype(jnp.bfloat16)
+    groups = router_group.shape[1]
+    if lax.axis_size("ep") == 2 * groups and lax.axis_size("tp") == 4:
+        moe_out = moe_by_group(
+            tokens_b,
+            moe_gain,
+            router_group,
+            router_expert,
+            route_expert,
+            expert_gate,
+            expert_up,
+            expert_down,
+        )
+        return (mixer_out, moe_out)
     tp_count = lax.axis_size("tp")
     tp_index = lax.axis_index("tp")
     exp_local = expert_gate.shape[0]

time: 385 us -> 115 us (0.30)
  waiting for transfers between devices: 239 us -> 0.02 us
  Pallas kernels: 0 us -> 72.1 us
  blocking collectives: 55.5 us -> 0 us
  matrix products: 30.1 us -> 9.46 us
  local copies, waits for them, and re-layouts: 24.9 us -> 7.97 us
  other arithmetic: 11.5 us -> 5.28 us
  starting transfers between devices: 9.2 us -> 4.93 us
    unnamed x4 -> x1, waiting for transfers between devices: 144 us -> 0.02 us
    pallas_call x0 -> x1, Pallas kernels: none -> 72.1 us  [moe_exchange(): pl.pallas_call(functools.partial(moe_kernel, groups), out_shape=jax.Shape...]
    all_gather x1 -> x0, waiting for transfers between devices: 57.4 us -> none  [per_device(): arrived = lax.all_gather(delivered, 'tp', axis=2, tiled=True)]
    all_to_all x1 -> x0, blocking collectives: 55.5 us -> none  [per_device(): lax.all_to_all(buffer, 'ep', split_axis=0, concat_axis=0, tiled=True)]
    all_gather x1, waiting for transfers between devices: 22.5 us -> 0.01 us  [per_device(): lax.all_gather(attended, 'tp', axis=1, tiled=True)]
    dot_general x2, matrix products: 21.2 us -> 1.44 us  [the longest x1 1.14 us: moe_by_group(): jnp.dot(put, result, preferred_element_type=jnp.float32)]
    all_to_all x1 -> x0, waiting for transfers between devices: 15.8 us -> none  [per_device(): lax.all_to_all(summed, 'ep', split_axis=0, concat_axis=0, tiled=True)]
    all_to_all x1 -> x0, starting transfers between devices: 5.52 us -> none  [per_device(): lax.all_to_all(summed, 'ep', split_axis=0, concat_axis=0, tiled=True)]
  transfers between devices with their start and end apart: 5 -> 2, of which waited for: 4 -> 0; matrix products, arithmetic and copies ran while one was open for 3% -> 9% of each run, Pallas kernels for 0% -> 63%
where the time goes in v1:
time: 115 us; the launch traced here: 114 us
  Pallas kernels  72.1 us (63%)
  between operations  14.4 us (13%)
  matrix products  9.46 us (8%)
  local copies, waits for them, and re-layouts  7.97 us (7%)
  other arithmetic  5.28 us (5%)
  starting transfers between devices  4.93 us (4%)
    pallas_call x1, Pallas kernels, moe_exchange(): pl.pallas_call(functools.partial(moe_kernel, groups), out_shape=jax.Shape...  72.1 us
    ppermute x1, starting transfers between devices, shifted(): lax.ppermute(value, axis, [(source, source + steps) for source in range(l...  4.89 us
    unnamed x17, local copies, waits for them, and re-layouts  4.18 us
    dot_general x1, matrix products, per_device(): jnp.dot(lax.all_gather(attended, 'tp', axis=1, tiled=True), out_weight, p...  3.84 us
  transfers between devices with their start and end apart: 2, of which 0 were waited for; matrix products, arithmetic and copies ran while one was open for 9% of the time, Pallas kernels for 63%

profile of v1, /device:TPU:0, one launch (start us, length us, event | category | flops | bytes accessed | tf_op | source)
XLA Modules:
  0.0 114.1 jit_solution(6452132128937502583)
XLA Ops:
  7.2 0.0 copy-start
  7.2 0.0 all-gather.2.cloned.1.call-start
  7.2 0.8 slice_bitcast_fusion.2
  8.1 4.9 %collective-permute-start = (bf16[2,128,64]{1,2,0:T(8,128)(2,1)S(1)}, bf16[2,128,64]{1,2,0:T(8,128)(2,1)S(1)}, u32[]{:S(2)}, u32[]{:S(2)}) collective-permute-start(bf16[2,128,64]{1,2,0:T(8,128)(2,1)S(1)} %pad_maximum_fusion.2), channel_id=1, source_target_pairs={{0,4},{4,8},{8,12},{12,16},{16,20},{20,24},{24,28},{1,5},{5,9},{9,... | collective-permute-start | bytes 98312 | tf_op jit(solution)/shard_map/ppermute | solution.py:19
  13.0 0.7 and_select_fusion
  13.7 0.1 add_compare_fusion
  13.9 1.2 %fusion.11 = f32[128]{0:T(128)S(1)} fusion(bf16[512,2048]{1,0:T(8,128)(2,1)} %param.18, s32[]{:T(128)S(6)} %select_n.45), kind=kLoop, calls=%fused_computation.15 | loop fusion | flops 786304 | bytes 524804 | tf_op jit(solution)/shard_map/reduce_sum | solution.py:24
  15.1 1.3 %fusion.13 = bf16[128,2048]{1,0:T(8,128)(2,1)S(1)} fusion(f32[2048]{0:T(1024)} %param.19, f32[128]{0:T(128)S(1)} %add_rsqrt_fusion, bf16[512,2048]{1,0:T(8,128)(2,1)} %param.18, s32[]{:T(128)S(6)} %select_n.45), kind=kLoop, calls=%fused_computation.17 | loop fusion | flops 1048576 | bytes 1057284 | tf_op jit(solution)/shard_map/convert_element_type | solution.py:25
  16.4 1.1 fusion.39
  17.5 1.0 fusion.38
  18.6 0.1 copy.39
  18.7 0.1 copy.40
  18.9 0.2 convert_reduce_fusion
  19.1 0.3 concatenate.19
  19.3 0.3 convolution_convert_fusion.xs_ref
  19.6 0.3 broadcast_and_fusion
  20.0 2.0 %reshape.242 = bf16[8,128,4,64]{3,2,1,0:T(4,128)(2,1)S(1)} reshape(bf16[1024,256]{1,0:T(8,128)(2,1)} %param.13) | data formatting | bytes 1048576 | tf_op jit(solution)/shard_map/reshape.15
  22.0 0.0 copy-start.5
  22.3 0.9 fusion.1
  23.2 0.1 broadcast_maximum_fusion
  23.3 1.1 fusion
  24.3 0.1 exponential_add_fusion
  24.5 1.2 %fusion.8 = bf16[8,128,1,4,64]{1,4,3,0,2:T(8,128)(2,1)S(1)} fusion(f32[8,4,128]{2,1,0:T(4,128)S(1)} %exponential_add_fusion, f32[8,4,128]{2,1,0:T(4,128)S(1)} %broadcast_maximum_fusion, f32[8,256,128,4]{2,1,3,0:T(8,128)S(1)} %get-tuple-element.9, pred[8,128,256]{1,2,0:T(8,128)(4,1)S(1)} %broadcast_and_fusion, bf16[8,128,1,64]{1,3,0,2:T(8,128)(2,1)S(1)} %copy.32, ...), kind=kOutput, calls=%fused_computation.14 | convolution fusion | flops 140247040 | bytes 5275648 | tf_op jit(solution)/shard_map/nhgqk,nkhd->nqhgd/dot_general | solution.py:402
  25.7 0.3 copy.38
  26.1 0.9 copy.56
  26.9 0.0 all-gather.2.cloned.1.call-update
  27.0 0.0 copy-start.1
  27.0 1.6 %copy-done.1 = bf16[2,2048,256]{2,1,0:T(8,128)(2,1)S(1)} copy-done((bf16[2,2048,256]{2,1,0:T(8,128)(2,1)S(1)}, bf16[2,2048,256]{2,1,0:T(8,128)(2,1)}, u32[]{:S(2)}) %copy-start.1) | copy-done | bytes 2097176
  28.6 1.6 %copy-done.2 = bf16[2,2048,256]{2,1,0:T(8,128)(2,1)S(1)} copy-done((bf16[2,2048,256]{2,1,0:T(8,128)(2,1)S(1)}, bf16[2,2048,256]{2,1,0:T(8,128)(2,1)}, u32[]{:S(2)}) %copy-start.2) | copy-done | bytes 2097176
  30.2 72.1 %shard_map.140 = bf16[128,2048]{1,0:T(8,128)(2,1)S(1)} custom-call(bf16[128,2176]{1,0:T(8,128)(2,1)S(1)} %convolution_convert_fusion.xs_ref, bf16[2,2048,256]{2,1,0:T(8,128)(2,1)S(1)} %copy-done.1, bf16[2,2048,256]{2,1,0:T(8,128)(2,1)S(1)} %copy-done.2, bf16[512,2048]{1,0:T(8,128)(2,1)} %bitcast.114), custom_call_target="tpu_custom_call" | custom-call | flops 60000002048 | bytes 200000000 | tf_op jit(solution)/shard_map/pallas_call | solution.py:276
  102.3 1.1 %convolution_convert_fusion.1 = bf16[128,2048]{1,0:T(8,128)(2,1)} fusion(bf16[128,2048]{1,0:T(8,128)(2,1)S(1)} %shard_map.140, s32[128]{0:T(128)S(1)} %fusion.33), kind=kOutput, calls=%fused_computation.6 | convolution fusion | flops 67387392 | bytes 1049088 | tf_op jit(solution)/shard_map/dot_general | solution.py:347
  103.4 3.8 %convolution_convert_fusion.2 = bf16[1024,512]{1,0:T(8,128)(2,1)} fusion(bf16[1024,1024]{0,1:T(8,128)(2,1)} %all-gather.2.cloned.1.call-done, bf16[1024,512]{1,0:T(8,128)(2,1)S(1)} %copy-done), kind=kOutput, calls=%fused_computation.10 | convolution fusion | flops 1074266112 | bytes 4194304 | tf_op jit(solution)/shard_map/dot_general | solution.py:406
  (37 shorter events, 0.5 us)
Async XLA Ops:
  7.2 96.2 %copy-start = (bf16[1024,512]{1,0:T(8,128)(2,1)S(1)}, bf16[1024,512]{1,0:T(8,128)(2,1)}, u32[]{:S(2)}) copy-start(bf16[1024,512]{1,0:T(8,128)(2,1)} %param.17) | copy-start | bytes 3145732
  7.2 14.9 %copy-start.3 = (bf16[1024,64]{0,1:T(8,128)(2,1)S(1)}, bf16[1024,64]{0,1:T(8,128)(2,1)}, u32[]{:S(2)}) copy-start(bf16[1024,64]{0,1:T(8,128)(2,1)} %param.14) | copy-start | bytes 393220
  7.2 14.9 %copy-start.4 = (bf16[1024,64]{0,1:T(8,128)(2,1)S(1)}, bf16[1024,64]{0,1:T(8,128)(2,1)}, u32[]{:S(2)}) copy-start(bf16[1024,64]{0,1:T(8,128)(2,1)} %param.15) | copy-start | bytes 393220
  7.2 96.2 %all-gather.2.cloned.1.call-start = ((), (), s32[]{:S(2)}) async-start(), calls=%async_computation | async-start | bytes 2621440 | tf_op jit(solution)/shard_map/all_gather | solution.py:407
  8.1 14.1 %collective-permute-start = (bf16[2,128,64]{1,2,0:T(8,128)(2,1)S(1)}, bf16[2,128,64]{1,2,0:T(8,128)(2,1)S(1)}, u32[]{:S(2)}, u32[]{:S(2)}) collective-permute-start(bf16[2,128,64]{1,2,0:T(8,128)(2,1)S(1)} %pad_maximum_fusion.2), channel_id=1, source_target_pairs={{0,4},{4,8},{8,12},{12,16},{16,20},{20,24},{24,28},{1,5},{5,9},{9,... | collective-permute-start | bytes 98312 | tf_op jit(solution)/shard_map/ppermute | solution.py:19
  22.0 1.2 %copy-start.5 = (f32[4]{0:T(128)S(1)}, f32[4]{0:T(128)}, u32[]{:S(2)}) copy-start(f32[4]{0:T(128)} %param.16) | copy-start | bytes 52
  27.0 1.6 %copy-start.1 = (bf16[2,2048,256]{2,1,0:T(8,128)(2,1)S(1)}, bf16[2,2048,256]{2,1,0:T(8,128)(2,1)}, u32[]{:S(2)}) copy-start(bf16[2,2048,256]{2,1,0:T(8,128)(2,1)} %gate_hbm.1) | copy-start | bytes 6291460
  28.6 1.6 %copy-start.2 = (bf16[2,2048,256]{2,1,0:T(8,128)(2,1)S(1)}, bf16[2,2048,256]{2,1,0:T(8,128)(2,1)}, u32[]{:S(2)}) copy-start(bf16[2,2048,256]{2,1,0:T(8,128)(2,1)} %up_hbm.1) | copy-start | bytes 6291460
Sparse Core Ops, SparseCore 0:
  27.1 25.2 all-gather.1

commit v2 on v0

--- a/solution.py
+++ b/solution.py
@@ -1,6 +1,10 @@
+import functools
+
 import jax
 import jax.numpy as jnp
 from jax import lax
+from jax.experimental import pallas as pl
+from jax.experimental.pallas import tpu as pltpu
 from jax.sharding import PartitionSpec as P
 
 HEADS = 16
@@ -54,6 +58,393 @@
     return buffer.reshape(
         expert_count // exp_local, exp_local, sub_count, capacity, normed.shape[1]
     )
+
+
+LANES = 128
+MESH = pl.DeviceIdType.MESH
+
+
+def fused_kernel(
+    groups,
+    sink_ref,
+    q_ref,
+    kv_ref,
+    xs_ref,
+    gate_hbm,
+    up_hbm,
+    down_hbm,
+    proj_hbm,
+    mixer_ref,
+    out_ref,
+    kv_ext,
+    heads,
+    rows,
+    part,
+    wg,
+    wu,
+    wd,
+    proj,
+    act,
+    from_core,
+    relay_x,
+    relay_y,
+    from_x,
+    from_y,
+    total,
+    back,
+    load_sem,
+    send_sem,
+    recv_sem,
+):
+    ep, tp = lax.axis_index("ep"), lax.axis_index("tp")
+    group, member = ep // 2, ep % 2
+    x, core = tp // 2, tp % 2
+    tp_x, tp_c = (1 - x) * 2 + core, x * 2 + (1 - core)
+    ep_y = group * 2 + (1 - member)
+    ep_count = groups * 2
+    x_dev, y_dev, c_dev = (ep, tp_x), (ep_y, tp), (ep, tp_c)
+    next_dev = ((ep + 1) % ep_count, tp)
+    prev_dev = ((ep + ep_count - 1) % ep_count, tp)
+    depth = out_ref.shape[1]
+    chunk = xs_ref.shape[0] // groups
+    half = chunk // 2
+    row_count = q_ref.shape[0]
+    lo, hi = pl.ds(0, half), pl.ds(half, half)
+    mine, other = core * 4, (1 - core) * 4
+    own = mine + member * 2 + x
+    slot_x = mine + member * 2 + (1 - x)
+    slot_y = mine + (1 - member) * 2 + x
+    slot_d = mine + (1 - member) * 2 + (1 - x)
+    mine_slots, other_slots = pl.ds(mine, 4), pl.ds(other, 4)
+
+    pairs = ((gate_hbm, wg), (up_hbm, wu), (down_hbm, wd), (proj_hbm, proj))
+    loads = [
+        pltpu.make_async_copy(source, held, load_sem.at[i])
+        for i, (source, held) in enumerate(pairs)
+    ]
+    for load in loads:
+        load.start()
+
+    barrier = pltpu.get_barrier_semaphore()
+    ahead = [((group + step) % groups) * 2 + member for step in range(1, groups)]
+    peers = [(plane, tp) for plane in ahead] + [x_dev, y_dev, c_dev, next_dev, prev_dev]
+    for peer in peers:
+        pl.semaphore_signal(barrier, inc=1, device_id=peer, device_id_type=MESH)
+    pl.semaphore_wait(barrier, len(peers))
+
+    started = []
+
+    def send(source, target, device):
+        index = len(started)
+        copy = pltpu.make_async_remote_copy(
+            src_ref=source,
+            dst_ref=target,
+            send_sem=send_sem.at[index],
+            recv_sem=recv_sem.at[index],
+            device_id=device,
+            device_id_type=MESH,
+        )
+        copy.start()
+        started.append(copy)
+        return copy
+
+    my_chunk = pl.ds(pl.multiple_of(group * chunk, chunk), chunk)
+    keep = pltpu.make_async_copy(xs_ref.at[my_chunk], rows.at[0, own], load_sem.at[4])
+    keep.start()
+    halo = send(kv_ref.at[pl.ds(row_count - WINDOW, WINDOW)], kv_ext.at[pl.ds(0, WINDOW)], next_dev)
+    z_out = [keep]
+    for step in range(1, groups):
+        plane = (group + step) % groups
+        there = pl.ds(pl.multiple_of(plane * chunk, chunk), chunk)
+        z_out.append(send(xs_ref.at[there], rows.at[step, own], (plane * 2 + member, tp)))
+    kv_ext[pl.ds(WINDOW, row_count)] = kv_ref[...]
+
+    held = [dict() for _ in range(groups)]
+
+    def stage_a(s):
+        if s:
+            z_out[s].wait_recv()
+        else:
+            keep.wait()
+        held[s]["x"] = send(rows.at[s, own], rows.at[s, own], x_dev)
+        held[s]["y"] = send(rows.at[s, own], rows.at[s, own], y_dev)
+
+    def stage_b(s):
+        held[s]["x"].wait_recv()
+        held[s]["to_y"] = send(rows.at[s, slot_x, lo], rows.at[s, slot_x, lo], y_dev)
+        held[s]["y"].wait_recv()
+        held[s]["to_x"] = send(rows.at[s, slot_y, hi], rows.at[s, slot_y, hi], x_dev)
+
+    def stage_c(s):
+        held[s]["to_y"].wait_recv()
+        held[s]["to_x"].wait_recv()
+        held[s]["core"] = send(rows.at[s, mine_slots], rows.at[s, mine_slots], c_dev)
+
+    def stage_d(s):
+        held[s]["core"].wait_recv()
+        batch = 8 * chunk
+        tokens = rows[s, :, :, :depth].reshape(batch, depth)
+        shares = rows[s, :, :, depth:].reshape(batch, LANES).astype(jnp.float32)
+        lane = lax.broadcasted_iota(jnp.int32, shares.shape, 1) % (LANES // 2)
+
+        def one(e, carry):
+            share = jnp.sum(
+                jnp.where(lane == member * wg.shape[0] + e, shares, 0.0), axis=1, keepdims=True
+            )
+            pre = jnp.dot(tokens, wg[e], preferred_element_type=jnp.float32)
+            up = jnp.dot(tokens, wu[e], preferred_element_type=jnp.float32)
+            act[e] = (jax.nn.silu(pre) * up * share).astype(jnp.bfloat16)
+            return carry
+
+        lax.fori_loop(0, wg.shape[0], one, 0)
+        acts = jnp.concatenate([act[e] for e in range(wg.shape[0])], axis=1)
+        tile = 512
+
+        def column(n, carry):
+            columns = pl.ds(pl.multiple_of(n * tile, tile), tile)
+            value = jnp.dot(acts, wd[:, columns], preferred_element_type=jnp.float32)
+            part[s, :, :, columns] = value.astype(jnp.bfloat16).reshape(8, chunk, tile)
+            return carry
+
+        lax.fori_loop(0, depth // tile, column, 0)
+        held[s]["sum"] = send(part.at[s, other_slots], from_core.at[s], c_dev)
+
+    def add(index, term):
+        part[index] = (part[index].astype(jnp.float32) + term.astype(jnp.float32)).astype(
+            jnp.bfloat16
+        )
+
+    def stage_e(s):
+        held[s]["sum"].wait_recv()
+        add((s, mine_slots), from_core[s])
+        held[s]["d_y"] = send(part.at[s, slot_d, lo], relay_y.at[s], y_dev)
+        held[s]["d_x"] = send(part.at[s, slot_d, hi], relay_x.at[s], x_dev)
+        held[s]["x_hi"] = send(part.at[s, slot_x, hi], from_x.at[s, hi], x_dev)
+        held[s]["y_lo"] = send(part.at[s, slot_y, lo], from_y.at[s, lo], y_dev)
+
+    def stage_f(s):
+        held[s]["d_y"].wait_recv()
+        add((s, slot_x, lo), relay_y[s])
+        held[s]["x_lo"] = send(part.at[s, slot_x, lo], from_x.at[s, lo], x_dev)
+        held[s]["d_x"].wait_recv()
+        add((s, slot_y, hi), relay_x[s])
+        held[s]["y_hi"] = send(part.at[s, slot_y, hi], from_y.at[s, hi], y_dev)
+
+    def stage_h(s):
+        for name in ("x_hi", "y_lo", "x_lo", "y_hi"):
+            held[s][name].wait_recv()
+        summed = (
+            part[s, own].astype(jnp.float32)
+            + from_x[s].astype(jnp.float32)
+            + from_y[s].astype(jnp.float32)
+        ).astype(jnp.bfloat16)
+        if s:
+            total[s] = summed
+            plane = (group + groups - s) % groups
+            held[s]["home"] = send(total.at[s], back.at[my_chunk], (plane * 2 + member, tp))
+        else:
+            back[my_chunk] = summed
+
+    head_count = q_ref.shape[1] // HD
+    query_at = lax.broadcasted_iota(jnp.int32, (WINDOW, 2 * WINDOW), 0)
+    key_at = lax.broadcasted_iota(jnp.int32, (WINDOW, 2 * WINDOW), 1)
+    distance = query_at + WINDOW - key_at
+    near = (distance >= 0) & (distance < WINDOW)
+
+    def attend(b, carry):
+        start = pl.multiple_of(b * WINDOW, WINDOW)
+        band = kv_ext[pl.ds(start, 2 * WINDOW)]
+        queries = q_ref[pl.ds(start, WINDOW)]
+        keys = band[:, :HD]
+        allowed = near & (key_at + (ep * row_count + b * WINDOW - WINDOW) >= 0)
+        outs = []
+        for h in range(head_count):
+            query = queries[:, h * HD : (h + 1) * HD]
+            scores = lax.dot_general(
+                query, keys, (((1,), (1,)), ((), ())), preferred_element_type=jnp.float32
+            ) * HD ** (-0.5)
+            masked = jnp.where(allowed, scores, -1e30)
+            sink = jnp.full((WINDOW, 1), sink_ref[h], jnp.float32)
+            row_max = jnp.maximum(jnp.max(masked, axis=1, keepdims=True), sink)
+            weights = jnp.exp(masked - row_max)
+            denominator = jnp.sum(weights, axis=1, keepdims=True) + jnp.exp(sink - row_max)
+            probs = (weights * (1.0 / denominator)).astype(jnp.bfloat16)
+            both = jnp.dot(probs, band, preferred_element_type=jnp.float32)
+            outs.append(both[:, HD:])
+        heads[tp, pl.ds(start, WINDOW)] = jnp.concatenate(outs, axis=1).astype(jnp.bfloat16)
+        return carry
+
+    blocks = row_count // WINDOW
+    piece = row_count // 4
+    att_x = []
+
+    def send_heads(i):
+        span = pl.ds(i * piece, piece)
+        att_x.append(send(heads.at[tp, span], heads.at[tp, span], x_dev))
+
+    stage_a(0)
+    lax.fori_loop(1, blocks // 2, attend, 0)
+    stage_b(0)
+    stage_a(1)
+    lax.fori_loop(blocks // 2, blocks, attend, 0)
+    stage_c(0)
+    stage_b(1)
+    stage_a(2)
+    halo.wait_recv()
+    lax.fori_loop(0, 1, attend, 0)
+    send_heads(0)
+    att_c = send(heads.at[tp], heads.at[tp], c_dev)
+    for load in loads:
+        load.wait()
+    stage_d(0)
+    stage_c(1)
+    stage_b(2)
+    stage_a(3)
+    stage_e(0)
+    stage_d(1)
+    send_heads(1)
+    stage_f(0)
+    stage_c(2)
+    stage_b(3)
+    stage_e(1)
+    stage_d(2)
+    stage_h(0)
+    send_heads(2)
+    stage_f(1)
+    stage_c(3)
+    stage_e(2)
+    stage_d(3)
+    stage_h(1)
+    stage_f(2)
+    stage_e(3)
+    send_heads(3)
+    stage_h(2)
+    stage_f(3)
+    for copy in att_x:
+        copy.wait_recv()
+    att_cx = send(heads.at[tp_x], heads.at[tp_x], c_dev)
+    att_c.wait_recv()
+    att_cx.wait_recv()
+    stage_h(3)
+
+    def project(i, carry):
+        span = pl.ds(pl.multiple_of(i * piece, piece), piece)
+        joined = jnp.concatenate([heads[t, span] for t in range(4)], axis=1)
+        mixer_ref[span] = jnp.dot(joined, proj[...], preferred_element_type=jnp.float32).astype(
+            jnp.bfloat16
+        )
+        return carry
+
+    lax.fori_loop(0, 4, project, 0)
+    for s in range(1, groups):
+        held[s]["home"].wait_recv()
+    out_ref[...] = back[...]
+    for copy in started:
+        copy.wait_send()
+
+
+def fused(sinks, q_heads, kv, sorted_rows, expert_gate, expert_up, expert_down, proj, groups):
+    block, width = sorted_rows.shape
+    experts, depth, hidden = expert_gate.shape
+    row_count, head_width = q_heads.shape
+    down = expert_down.reshape(experts * hidden, depth)
+    chunk = block // groups
+    copies = 14 * groups + 8
+    bf16 = jnp.bfloat16
+    anywhere = pl.BlockSpec(memory_space=pl.ANY)
+    vmem = pl.BlockSpec(memory_space=pltpu.VMEM)
+    return pl.pallas_call(
+        functools.partial(fused_kernel, groups),
+        out_shape=(
+            jax.ShapeDtypeStruct((row_count, proj.shape[1]), bf16),
+            jax.ShapeDtypeStruct((block, depth), bf16),
+        ),
+        in_specs=[pl.BlockSpec(memory_space=pltpu.SMEM), vmem, vmem, vmem] + [anywhere] * 4,
+        out_specs=(vmem, vmem),
+        scratch_shapes=[
+            pltpu.VMEM((row_count + WINDOW, 2 * HD), bf16),
+            pltpu.VMEM((4, row_count, head_width), bf16),
+            pltpu.VMEM((groups, 8, chunk, width), bf16),
+            pltpu.VMEM((groups, 8, chunk, depth), bf16),
+            pltpu.VMEM(expert_gate.shape, bf16),
+            pltpu.VMEM(expert_up.shape, bf16),
+            pltpu.VMEM(down.shape, bf16),
+            pltpu.VMEM(proj.shape, bf16),
+            pltpu.VMEM((experts, 8 * chunk, hidden), bf16),
+            pltpu.VMEM((groups, 4, chunk, depth), bf16),
+            pltpu.VMEM((groups, chunk // 2, depth), bf16),
+            pltpu.VMEM((groups, chunk // 2, depth), bf16),
+            pltpu.VMEM((groups, chunk, depth), bf16),
+            pltpu.VMEM((groups, chunk, depth), bf16),
+            pltpu.VMEM((groups, chunk, depth), bf16),
+            pltpu.VMEM((block, depth), bf16),
+            pltpu.SemaphoreType.DMA((5,)),
+            pltpu.SemaphoreType.DMA((copies,)),
+            pltpu.SemaphoreType.DMA((copies,)),
+        ],
+        cost_estimate=pl.CostEstimate(
+            flops=20_000_000_000, bytes_accessed=20_000_000, transcendentals=0
+        ),
+        compiler_params=pltpu.CompilerParams(
+            collective_id=0, has_side_effects=True, vmem_limit_bytes=56 * 2**20
+        ),
+    )(sinks, q_heads, kv, sorted_rows, expert_gate, expert_up, down, proj)
+
+
+def by_group(
+    q_heads,
+    k_heads,
+    v_heads,
+    sink_logits,
+    out_weight,
+    tokens_b,
+    moe_gain,
+    router_group,
+    router_expert,
+    route_expert,
+    expert_gate,
+    expert_up,
+    expert_down,
+):
+    tp_count = lax.axis_size("tp")
+    tp_index = lax.axis_index("tp")
+    groups = router_group.shape[1]
+    group_experts = router_expert.shape[1] // groups
+    rows_dev = tokens_b.shape[0] // tp_count
+    routes = lax.dynamic_slice_in_dim(route_expert, tp_index * rows_dev, rows_dev, 0)
+    normed = normalize(
+        lax.dynamic_slice_in_dim(tokens_b, tp_index * rows_dev, rows_dev, 0), moe_gain
+    )
+    gates = gate_weights(normed, routes, router_group, router_expert)
+    lanes = jnp.arange(LANES // 2, dtype=jnp.int32)
+    share = jnp.sum(
+        jnp.where((routes % group_experts)[:, :, None] == lanes, gates[:, :, None], 0.0), axis=1
+    )
+    coarse = lax.reduce_precision(share, 8, 7)
+    extended = jnp.concatenate(
+        [normed, coarse.astype(jnp.bfloat16), (share - coarse).astype(jnp.bfloat16)], axis=1
+    )
+    named = routes[:, 0] // group_experts
+    same = named[:, None] == named[None, :]
+    order = jnp.arange(rows_dev, dtype=jnp.int32)
+    rank = jnp.sum((same & (order[None, :] < order[:, None])).astype(jnp.int32), axis=1)
+    place = named * (rows_dev // groups) + rank
+    take = (place[None, :] == order[:, None]).astype(jnp.bfloat16)
+    put = (place[:, None] == order[None, :]).astype(jnp.bfloat16)
+    sorted_rows = jnp.dot(take, extended, preferred_element_type=jnp.float32)
+    mixer_out, result = fused(
+        sink_logits,
+        q_heads,
+        jnp.concatenate([k_heads, v_heads], axis=1),
+        sorted_rows.astype(jnp.bfloat16),
+        expert_gate,
+        expert_up,
+        expert_down,
+        out_weight,
+        groups,
+    )
+    moe_out = jnp.dot(put, result, preferred_element_type=jnp.float32).astype(jnp.bfloat16)
+    return (mixer_out, moe_out)
 
 
 def per_device(
@@ -71,6 +462,23 @@
     expert_up,
     expert_down,
 ):
+    groups = router_group.shape[1]
+    if (lax.axis_size("ep"), lax.axis_size("tp"), k_heads.shape[1]) == (2 * groups, 4, HD):
+        return by_group(
+            q_heads,
+            k_heads,
+            v_heads,
+            sink_logits,
+            out_weight,
+            tokens_b,
+            moe_gain,
+            router_group,
+            router_expert,
+            route_expert,
+            expert_gate,
+            expert_up,
+            expert_down,
+        )
     span_len = WINDOW
     row_count = q_heads.shape[0]
     kv_local = k_heads.shape[1] // HD

time: 385 us -> 80.7 us (0.21)
  waiting for transfers between devices: 239 us -> 0 us
  Pallas kernels: 0 us -> 66.5 us
  blocking collectives: 55.5 us -> 0 us
  matrix products: 30.1 us -> 3.78 us
  local copies, waits for them, and re-layouts: 24.9 us -> 4.93 us
  between operations: 14.1 us -> 0.79 us
  starting transfers between devices: 9.2 us -> 0 us
  other arithmetic: 11.5 us -> 4.43 us
    unnamed x4 -> x0, waiting for transfers between devices: 144 us -> none
    all_gather x2 -> x0, waiting for transfers between devices: 79.9 us -> none  [the longest x1 57.4 us: per_device(): arrived = lax.all_gather(delivered, 'tp', axis=2, tiled=True)]
    pallas_call x0 -> x1, Pallas kernels: none -> 66.5 us  [fused(): pl.pallas_call(functools.partial(fused_kernel, groups), out_shape=(jax.Sh...]
    all_to_all x1 -> x0, blocking collectives: 55.5 us -> none  [per_device(): lax.all_to_all(buffer, 'ep', split_axis=0, concat_axis=0, tiled=True)]
    dot_general x5 -> x2, matrix products: 29.6 us -> 3.29 us  [the longest x1 2.18 us: by_group(): jnp.dot(put, result, preferred_element_type=jnp.float32)]
    all_to_all x1 -> x0, waiting for transfers between devices: 15.8 us -> none  [per_device(): lax.all_to_all(summed, 'ep', split_axis=0, concat_axis=0, tiled=True)]
    reduce_sum x3 -> x2, other arithmetic: 6.69 us -> 0.19 us  [the longest x1 0.17 us: by_group(): jnp.sum((same & (order[None, :] < order[:, None])).astype(jnp.int32), axi...]
    all_to_all x1 -> x0, starting transfers between devices: 5.52 us -> none  [per_device(): lax.all_to_all(summed, 'ep', split_axis=0, concat_axis=0, tiled=True)]
  transfers between devices with their start and end apart: 5 -> 0, of which waited for: 4 -> 0; matrix products, arithmetic and copies ran while one was open for 3% -> 0% of each run, Pallas kernels for 0% -> 0%
where the time goes in v2:
time: 80.7 us; the launch traced here: 80.4 us
  Pallas kernels  66.5 us (82%)
  local copies, waits for them, and re-layouts  4.93 us (6%)
  other arithmetic  4.43 us (5%)
  matrix products  3.78 us (5%)
    pallas_call x1, Pallas kernels, fused(): pl.pallas_call(functools.partial(fused_kernel, groups), out_shape=(jax.Sh...  66.5 us
    unnamed x9, local copies, waits for them, and re-layouts  4.43 us
    dot_general x1, matrix products, by_group(): jnp.dot(put, result, preferred_element_type=jnp.float32)  2.18 us

profile of v2, /device:TPU:0, one launch (start us, length us, event | category | flops | bytes accessed | tf_op | source)
XLA Modules:
  0.0 80.4 jit_solution(14526312490241143235)
XLA Ops:
  0.6 0.0 copy-start
  0.6 0.0 copy-start.1
  0.7 0.0 copy-start.2
  0.7 1.3 %fusion = f32[128]{0:T(128)S(1)} fusion(bf16[512,2048]{1,0:T(8,128)(2,1)} %param.18, s32[]{:T(128)S(6)} %select_n.40), kind=kLoop, calls=%fused_computation.4 | loop fusion | flops 786304 | bytes 524804 | tf_op jit(solution)/shard_map/reduce_sum | solution.py:24
  1.9 0.7 and_select_fusion
  2.7 0.2 convert_reduce_fusion
  2.9 1.1 %copy.20 = bf16[1024,64]{1,0:T(8,128)(2,1)S(1)} copy(bf16[1024,64]{0,1:T(8,128)(2,1)} %param.14) | data formatting | bytes 262144 | tf_op args[1]
  4.0 1.1 %copy.21 = bf16[1024,64]{1,0:T(8,128)(2,1)S(1)} copy(bf16[1024,64]{0,1:T(8,128)(2,1)} %param.15) | data formatting | bytes 262144 | tf_op args[2]
  5.0 0.9 %pad_maximum_fusion.kv_ref = bf16[1024,128]{1,0:T(8,128)(2,1)} fusion(bf16[1024,64]{1,0:T(8,128)(2,1)S(1)} %copy.21, bf16[1024,64]{1,0:T(8,128)(2,1)S(1)} %copy.20), kind=kLoop, calls=%fused_computation.7 | loop fusion | flops 524288 | bytes 524288 | tf_op jit(solution)/shard_map/concatenate | solution.py:438
  5.9 0.0 copy-done.2
  5.9 1.2 %fusion.2 = bf16[128,2048]{1,0:T(8,128)(2,1)S(1)} fusion(f32[2048]{0:T(1024)S(1)} %copy-done.2, f32[128]{0:T(128)S(1)} %add_rsqrt_fusion, bf16[512,2048]{1,0:T(8,128)(2,1)} %param.18, s32[]{:T(128)S(6)} %select_n.40), kind=kLoop, calls=%fused_computation.6 | loop fusion | flops 1048576 | bytes 1057284 | tf_op jit(solution)/shard_map/convert_element_type | solution.py:25
  7.1 0.0 copy-done.1
  7.1 0.2 fusion.12
  7.5 0.0 copy-done
  7.5 0.2 fusion.13
  7.8 0.1 copy.23
  8.0 0.1 copy.22
  8.1 0.3 concatenate.7
  8.4 1.1 %convolution_convert_fusion.xs_ref = bf16[128,2176]{1,0:T(8,128)(2,1)} fusion(bf16[128,2176]{1,0:T(8,128)(2,1)S(1)} %concatenate.7, s32[128]{0:T(128)S(1)} %multiply_add_fusion), kind=kOutput, calls=%fused_computation | convolution fusion | flops 71598080 | bytes 1114624 | tf_op jit(solution)/shard_map/dot_general | solution.py:434
  9.5 66.5 %shard_map.140 = (bf16[1024,512]{1,0:T(8,128)(2,1)}, bf16[128,2048]{1,0:T(8,128)(2,1)}) custom-call(f32[4]{0:T(128)} %sink_ref.1, bf16[1024,256]{1,0:T(8,128)(2,1)} %q_ref.1, bf16[1024,128]{1,0:T(8,128)(2,1)} %pad_maximum_fusion.kv_ref, bf16[128,2176]{1,0:T(8,128)(2,1)} %convolution_convert_fusion.xs_ref, bf16[2,2048,256]{2,1,0:T(8,128)(2,1)} %gate_hbm.1, ...), custom_call_target="tpu_custom_call" | custom-call | flops 20000000000 | bytes 20000000 | tf_op jit(solution)/shard_map/pallas_call | solution.py:356
  75.9 2.2 %convolution_convert_fusion.1 = bf16[128,2048]{1,0:T(8,128)(2,1)} fusion(bf16[128,2048]{1,0:T(8,128)(2,1)} %get-tuple-element.5, s32[128]{0:T(128)S(1)} %fusion.11), kind=kOutput, calls=%fused_computation.1 | convolution fusion | flops 67387392 | bytes 1049088 | tf_op jit(solution)/shard_map/dot_general | solution.py:446
  78.1 2.3 %copy.25 = bf16[1024,512]{1,0:T(8,128)(2,1)} copy(bf16[1024,512]{1,0:T(8,128)(2,1)} %get-tuple-element.14) | data formatting | bytes 2097152
  (13 shorter events, 0.2 us)
Async XLA Ops:
  0.6 6.8 %copy-start = (bf16[2048,16]{0,1:T(8,128)(2,1)S(1)}, bf16[2048,16]{0,1:T(8,128)(2,1)}, u32[]{:S(2)}) copy-start(bf16[2048,16]{0,1:T(8,128)(2,1)} %param.21) | copy-start | bytes 196612
  0.6 6.5 %copy-start.1 = (bf16[2048,4]{0,1:T(4,128)(2,1)S(1)}, bf16[2048,4]{0,1:T(4,128)(2,1)}, u32[]{:S(2)}) copy-start(bf16[2048,4]{0,1:T(4,128)(2,1)} %param.20) | copy-start | bytes 49156
  0.7 5.2 %copy-start.2 = (f32[2048]{0:T(1024)S(1)}, f32[2048]{0:T(1024)}, u32[]{:S(2)}) copy-start(f32[2048]{0:T(1024)} %param.19) | copy-start | bytes 24580

commit v3 on v2

--- a/solution.py
+++ b/solution.py
@@ -68,15 +68,23 @@
     groups,
     sink_ref,
     q_ref,
-    kv_ref,
-    xs_ref,
+    k_ref,
+    v_ref,
+    gain_ref,
+    group_ref,
+    expert_ref,
+    route_ref,
+    tokens_hbm,
     gate_hbm,
     up_hbm,
     down_hbm,
     proj_hbm,
     mixer_ref,
     out_ref,
-    kv_ext,
+    k_ext,
+    v_ext,
+    tokens,
+    xs_ref,
     heads,
     rows,
     part,
@@ -122,6 +130,10 @@
         pltpu.make_async_copy(source, held, load_sem.at[i])
         for i, (source, held) in enumerate(pairs)
     ]
+    block = xs_ref.shape[0]
+    first = pl.multiple_of(tp * block, block)
+    fetch = pltpu.make_async_copy(tokens_hbm.at[pl.ds(first, block)], tokens, load_sem.at[5])
+    fetch.start()
     for load in loads:
         load.start()
 
@@ -130,6 +142,56 @@
     peers = [(plane, tp) for plane in ahead] + [x_dev, y_dev, c_dev, next_dev, prev_dev]
     for peer in peers:
         pl.semaphore_signal(barrier, inc=1, device_id=peer, device_id_type=MESH)
+    fetch.wait()
+    values = tokens[...].astype(jnp.float32)
+    scale = lax.rsqrt(jnp.mean(values * values, axis=1, keepdims=True) + 1e-06)
+    normed = (values * scale * gain_ref[...]).astype(jnp.bfloat16)
+    across = (((1,), (1,)), ((), ()))
+    group_logits = lax.dot_general(
+        group_ref[...], normed, across, preferred_element_type=jnp.float32
+    )
+    expert_logits = lax.dot_general(
+        expert_ref[...], normed, across, preferred_element_type=jnp.float32
+    )
+    routes = route_ref[:, pl.ds(first, block)]
+    route_a, route_b = routes[0:1], routes[1:2]
+    group_experts = expert_ref.shape[0] // groups
+    group_at = lax.broadcasted_iota(jnp.int32, (groups, block), 0)
+    inside = route_a - group_at * group_experts
+    named = (inside >= 0) & (inside < group_experts)
+    group_exp = jnp.exp(group_logits - jnp.max(group_logits, axis=0, keepdims=True))
+    group_share = jnp.sum(jnp.where(named, group_exp, 0.0), axis=0, keepdims=True) / jnp.sum(
+        group_exp, axis=0, keepdims=True
+    )
+    expert_at = lax.broadcasted_iota(jnp.int32, expert_logits.shape, 0)
+    logit_a = jnp.sum(jnp.where(expert_at == route_a, expert_logits, 0.0), axis=0, keepdims=True)
+    logit_b = jnp.sum(jnp.where(expert_at == route_b, expert_logits, 0.0), axis=0, keepdims=True)
+    top = jnp.maximum(logit_a, logit_b)
+    exp_a, exp_b = jnp.exp(logit_a - top), jnp.exp(logit_b - top)
+    gate_a = group_share * (exp_a / (exp_a + exp_b))
+    gate_b = group_share * (exp_b / (exp_a + exp_b))
+    base = jnp.sum(jnp.where(named, group_at * group_experts, 0), axis=0, keepdims=True)
+    lane_at = lax.broadcasted_iota(jnp.int32, (LANES // 2, block), 0)
+    share_t = jnp.where(lane_at == route_a - base, gate_a, 0.0) + jnp.where(
+        lane_at == route_b - base, gate_b, 0.0
+    )
+    coarse = share_t.astype(jnp.bfloat16)
+    fine = (share_t - coarse.astype(jnp.float32)).astype(jnp.bfloat16)
+    row_at = lax.broadcasted_iota(jnp.int32, (block, block), 0)
+    column_at = lax.broadcasted_iota(jnp.int32, (block, block), 1)
+    earlier = jnp.where(row_at < column_at, 1.0, 0.0).astype(jnp.bfloat16)
+    counts = jnp.dot(
+        jnp.where(named, 1.0, 0.0).astype(jnp.bfloat16), earlier, preferred_element_type=jnp.float32
+    )
+    first_row = (group_at * chunk).astype(jnp.float32)
+    place = jnp.sum(jnp.where(named, counts + first_row, 0.0), axis=0, keepdims=True)
+    take = jnp.where(row_at.astype(jnp.float32) == place, 1.0, 0.0).astype(jnp.bfloat16)
+    xs_ref[:, :depth] = jnp.dot(take, normed, preferred_element_type=jnp.float32).astype(
+        jnp.bfloat16
+    )
+    xs_ref[:, depth:] = lax.dot_general(
+        take, jnp.concatenate([coarse, fine], axis=0), across, preferred_element_type=jnp.float32
+    ).astype(jnp.bfloat16)
     pl.semaphore_wait(barrier, len(peers))
 
     started = []
@@ -151,13 +213,18 @@
     my_chunk = pl.ds(pl.multiple_of(group * chunk, chunk), chunk)
     keep = pltpu.make_async_copy(xs_ref.at[my_chunk], rows.at[0, own], load_sem.at[4])
     keep.start()
-    halo = send(kv_ref.at[pl.ds(row_count - WINDOW, WINDOW)], kv_ext.at[pl.ds(0, WINDOW)], next_dev)
+    tail = pl.ds(row_count - WINDOW, WINDOW)
+    halo = [
+        send(source.at[:, tail], target.at[:, pl.ds(0, WINDOW)], next_dev)
+        for source, target in ((k_ref, k_ext), (v_ref, v_ext))
+    ]
     z_out = [keep]
     for step in range(1, groups):
         plane = (group + step) % groups
         there = pl.ds(pl.multiple_of(plane * chunk, chunk), chunk)
         z_out.append(send(xs_ref.at[there], rows.at[step, own], (plane * 2 + member, tp)))
-    kv_ext[pl.ds(WINDOW, row_count)] = kv_ref[...]
+    k_ext[:, pl.ds(WINDOW, row_count)] = k_ref[...]
+    v_ext[:, pl.ds(WINDOW, row_count)] = v_ref[...]
 
     held = [dict() for _ in range(groups)]
 
@@ -171,13 +238,11 @@
 
     def stage_b(s):
         held[s]["x"].wait_recv()
-        held[s]["to_y"] = send(rows.at[s, slot_x, lo], rows.at[s, slot_x, lo], y_dev)
+        held[s]["to_y"] = send(rows.at[s, slot_x], rows.at[s, slot_x], y_dev)
+
+    def stage_c(s):
         held[s]["y"].wait_recv()
-        held[s]["to_x"] = send(rows.at[s, slot_y, hi], rows.at[s, slot_y, hi], x_dev)
-
-    def stage_c(s):
         held[s]["to_y"].wait_recv()
-        held[s]["to_x"].wait_recv()
         held[s]["core"] = send(rows.at[s, mine_slots], rows.at[s, mine_slots], c_dev)
 
     def stage_d(s):
@@ -253,24 +318,21 @@
 
     def attend(b, carry):
         start = pl.multiple_of(b * WINDOW, WINDOW)
-        band = kv_ext[pl.ds(start, 2 * WINDOW)]
+        keys = k_ext[:, pl.ds(start, 2 * WINDOW)]
+        band = v_ext[:, pl.ds(start, 2 * WINDOW)]
         queries = q_ref[pl.ds(start, WINDOW)]
-        keys = band[:, :HD]
         allowed = near & (key_at + (ep * row_count + b * WINDOW - WINDOW) >= 0)
         outs = []
         for h in range(head_count):
             query = queries[:, h * HD : (h + 1) * HD]
-            scores = lax.dot_general(
-                query, keys, (((1,), (1,)), ((), ())), preferred_element_type=jnp.float32
-            ) * HD ** (-0.5)
+            scores = jnp.dot(query, keys, preferred_element_type=jnp.float32) * HD ** (-0.5)
             masked = jnp.where(allowed, scores, -1e30)
             sink = jnp.full((WINDOW, 1), sink_ref[h], jnp.float32)
             row_max = jnp.maximum(jnp.max(masked, axis=1, keepdims=True), sink)
             weights = jnp.exp(masked - row_max)
             denominator = jnp.sum(weights, axis=1, keepdims=True) + jnp.exp(sink - row_max)
             probs = (weights * (1.0 / denominator)).astype(jnp.bfloat16)
-            both = jnp.dot(probs, band, preferred_element_type=jnp.float32)
-            outs.append(both[:, HD:])
+            outs.append(lax.dot_general(probs, band, across, preferred_element_type=jnp.float32))
         heads[tp, pl.ds(start, WINDOW)] = jnp.concatenate(outs, axis=1).astype(jnp.bfloat16)
         return carry
 
@@ -290,7 +352,8 @@
     stage_c(0)
     stage_b(1)
     stage_a(2)
-    halo.wait_recv()
+    for copy in halo:
+        copy.wait_recv()
     lax.fori_loop(0, 1, attend, 0)
     send_heads(0)
     att_c = send(heads.at[tp], heads.at[tp], c_dev)
@@ -338,14 +401,32 @@
     lax.fori_loop(0, 4, project, 0)
     for s in range(1, groups):
         held[s]["home"].wait_recv()
-    out_ref[...] = back[...]
+    out_ref[...] = lax.dot_general(
+        take, back[...], (((0,), (0,)), ((), ())), preferred_element_type=jnp.float32
+    ).astype(jnp.bfloat16)
     for copy in started:
         copy.wait_send()
 
 
-def fused(sinks, q_heads, kv, sorted_rows, expert_gate, expert_up, expert_down, proj, groups):
-    block, width = sorted_rows.shape
+def fused(
+    sinks,
+    q_heads,
+    k_heads,
+    v_heads,
+    gain,
+    router_group,
+    router_expert,
+    routes,
+    tokens_b,
+    expert_gate,
+    expert_up,
+    expert_down,
+    proj,
+):
+    groups = router_group.shape[1]
+    block = tokens_b.shape[0] // 4
     experts, depth, hidden = expert_gate.shape
+    width = depth + LANES
     row_count, head_width = q_heads.shape
     down = expert_down.reshape(experts * hidden, depth)
     chunk = block // groups
@@ -359,10 +440,13 @@
             jax.ShapeDtypeStruct((row_count, proj.shape[1]), bf16),
             jax.ShapeDtypeStruct((block, depth), bf16),
         ),
-        in_specs=[pl.BlockSpec(memory_space=pltpu.SMEM), vmem, vmem, vmem] + [anywhere] * 4,
+        in_specs=[pl.BlockSpec(memory_space=pltpu.SMEM)] + [vmem] * 7 + [anywhere] * 5,
         out_specs=(vmem, vmem),
         scratch_shapes=[
-            pltpu.VMEM((row_count + WINDOW, 2 * HD), bf16),
+            pltpu.VMEM((HD, row_count + WINDOW), bf16),
+            pltpu.VMEM((HD, row_count + WINDOW), bf16),
+            pltpu.VMEM((block, depth), bf16),
+            pltpu.VMEM((block, width), bf16),
             pltpu.VMEM((4, row_count, head_width), bf16),
             pltpu.VMEM((groups, 8, chunk, width), bf16),
             pltpu.VMEM((groups, 8, chunk, depth), bf16),
@@ -378,7 +462,7 @@
             pltpu.VMEM((groups, chunk, depth), bf16),
             pltpu.VMEM((groups, chunk, depth), bf16),
             pltpu.VMEM((block, depth), bf16),
-            pltpu.SemaphoreType.DMA((5,)),
+            pltpu.SemaphoreType.DMA((6,)),
             pltpu.SemaphoreType.DMA((copies,)),
             pltpu.SemaphoreType.DMA((copies,)),
         ],
@@ -388,63 +472,21 @@
         compiler_params=pltpu.CompilerParams(
             collective_id=0, has_side_effects=True, vmem_limit_bytes=56 * 2**20
         ),
-    )(sinks, q_heads, kv, sorted_rows, expert_gate, expert_up, down, proj)
-
-
-def by_group(
-    q_heads,
-    k_heads,
-    v_heads,
-    sink_logits,
-    out_weight,
-    tokens_b,
-    moe_gain,
-    router_group,
-    router_expert,
-    route_expert,
-    expert_gate,
-    expert_up,
-    expert_down,
-):
-    tp_count = lax.axis_size("tp")
-    tp_index = lax.axis_index("tp")
-    groups = router_group.shape[1]
-    group_experts = router_expert.shape[1] // groups
-    rows_dev = tokens_b.shape[0] // tp_count
-    routes = lax.dynamic_slice_in_dim(route_expert, tp_index * rows_dev, rows_dev, 0)
-    normed = normalize(
-        lax.dynamic_slice_in_dim(tokens_b, tp_index * rows_dev, rows_dev, 0), moe_gain
-    )
-    gates = gate_weights(normed, routes, router_group, router_expert)
-    lanes = jnp.arange(LANES // 2, dtype=jnp.int32)
-    share = jnp.sum(
-        jnp.where((routes % group_experts)[:, :, None] == lanes, gates[:, :, None], 0.0), axis=1
-    )
-    coarse = lax.reduce_precision(share, 8, 7)
-    extended = jnp.concatenate(
-        [normed, coarse.astype(jnp.bfloat16), (share - coarse).astype(jnp.bfloat16)], axis=1
-    )
-    named = routes[:, 0] // group_experts
-    same = named[:, None] == named[None, :]
-    order = jnp.arange(rows_dev, dtype=jnp.int32)
-    rank = jnp.sum((same & (order[None, :] < order[:, None])).astype(jnp.int32), axis=1)
-    place = named * (rows_dev // groups) + rank
-    take = (place[None, :] == order[:, None]).astype(jnp.bfloat16)
-    put = (place[:, None] == order[None, :]).astype(jnp.bfloat16)
-    sorted_rows = jnp.dot(take, extended, preferred_element_type=jnp.float32)
-    mixer_out, result = fused(
-        sink_logits,
+    )(
+        sinks,
         q_heads,
-        jnp.concatenate([k_heads, v_heads], axis=1),
-        sorted_rows.astype(jnp.bfloat16),
+        k_heads.T,
+        v_heads.T,
+        gain[None, :],
+        router_group.T,
+        router_expert.T,
+        routes.T,
+        tokens_b,
         expert_gate,
         expert_up,
-        expert_down,
-        out_weight,
-        groups,
-    )
-    moe_out = jnp.dot(put, result, preferred_element_type=jnp.float32).astype(jnp.bfloat16)
-    return (mixer_out, moe_out)
+        down,
+        proj,
+    )
 
 
 def per_device(
@@ -464,20 +506,20 @@
 ):
     groups = router_group.shape[1]
     if (lax.axis_size("ep"), lax.axis_size("tp"), k_heads.shape[1]) == (2 * groups, 4, HD):
-        return by_group(
+        return fused(
+            sink_logits,
             q_heads,
             k_heads,
             v_heads,
-            sink_logits,
-            out_weight,
-            tokens_b,
             moe_gain,
             router_group,
             router_expert,
             route_expert,
+            tokens_b,
             expert_gate,
             expert_up,
             expert_down,
+            out_weight,
         )
     span_len = WINDOW
     row_count = q_heads.shape[0]

time: 80.7 us -> 69.1 us (0.86)
  other arithmetic: 4.43 us -> 0 us
  matrix products: 3.78 us -> 0 us
  local copies, waits for them, and re-layouts: 4.93 us -> 3.12 us
  Pallas kernels: 66.5 us -> 65.1 us
    dot_general x4 -> x0, matrix products: 3.78 us -> none  [the longest x1 2.18 us: by_group(): jnp.dot(put, result, preferred_element_type=jnp.float32)]
    reduce_sum x7 -> x0, other arithmetic: 1.56 us -> none  [the longest x1 1.26 us: normalize(): jnp.mean(values * values, axis=-1, keepdims=True) + 1e-06]
    pallas_call x1, Pallas kernels: 66.5 us -> 65.1 us  [fused(): pl.pallas_call(functools.partial(fused_kernel, groups), out_shape=(jax.Sh...]
    unnamed x9 -> x4, local copies, waits for them, and re-layouts: 4.43 us -> 3.12 us
    convert_element_type x2 -> x0, other arithmetic: 1.24 us -> none  [the longest x1 1.23 us: normalize(): return scaled.astype(jnp.bfloat16)]
    concatenate x1 -> x0, other arithmetic: 0.85 us -> none  [by_group(): jnp.concatenate([k_heads, v_heads], axis=1)]
where the time goes in v3:
time: 69.1 us; the launch traced here: 68.9 us
  Pallas kernels  65.1 us (94%)
  local copies, waits for them, and re-layouts  3.12 us (5%)
    pallas_call x1, Pallas kernels, fused(): pl.pallas_call(functools.partial(fused_kernel, groups), out_shape=(jax.Sh...  65.1 us
    unnamed x4, local copies, waits for them, and re-layouts  3.12 us

profile of v3, /device:TPU:0, one launch (start us, length us, event | category | flops | bytes accessed | tf_op | source)
XLA Modules:
  0.0 68.9 jit_solution(522516714036971327)
XLA Ops:
  0.6 65.1 %shard_map.140 = (bf16[1024,512]{1,0:T(8,128)(2,1)}, bf16[128,2048]{1,0:T(8,128)(2,1)}) custom-call(f32[4]{0:T(128)} %sink_ref.1, bf16[1024,256]{1,0:T(8,128)(2,1)} %q_ref.1, bf16[64,1024]{1,0:T(8,128)(2,1)} %bitcast.8, bf16[64,1024]{1,0:T(8,128)(2,1)} %bitcast.9, f32[1,2048]{1,0:T(1,128)} %bitcast.12, bf16[4,2048]{1,0:T(4,128)(2,1)} %bitcast.11, ...), custom_call_target="tpu_custom_call" | custom-call | flops 20000000000 | bytes 20000000 | tf_op jit(solution)/shard_map/pallas_call | solution.py:437
  65.8 0.0 copy-start
  65.8 2.3 %copy.17 = bf16[1024,512]{1,0:T(8,128)(2,1)} copy(bf16[1024,512]{1,0:T(8,128)(2,1)} %get-tuple-element.4) | data formatting | bytes 2097152
  68.1 0.0 copy-done
  68.1 0.8 %copy.18 = bf16[128,2048]{1,0:T(8,128)(2,1)} copy(bf16[128,2048]{1,0:T(8,128)(2,1)S(1)} %copy-done) | data formatting | bytes 1048576
Async XLA Ops:
  65.8 2.3 %copy-start = (bf16[128,2048]{1,0:T(8,128)(2,1)S(1)}, bf16[128,2048]{1,0:T(8,128)(2,1)}, u32[]{:S(2)}) copy-start(bf16[128,2048]{1,0:T(8,128)(2,1)} %get-tuple-element.5) | copy-start | bytes 1572868

commit v4 on v3

--- a/solution.py
+++ b/solution.py
@@ -352,44 +352,6 @@
     stage_c(0)
     stage_b(1)
     stage_a(2)
-    for copy in halo:
-        copy.wait_recv()
-    lax.fori_loop(0, 1, attend, 0)
-    send_heads(0)
-    att_c = send(heads.at[tp], heads.at[tp], c_dev)
-    for load in loads:
-        load.wait()
-    stage_d(0)
-    stage_c(1)
-    stage_b(2)
-    stage_a(3)
-    stage_e(0)
-    stage_d(1)
-    send_heads(1)
-    stage_f(0)
-    stage_c(2)
-    stage_b(3)
-    stage_e(1)
-    stage_d(2)
-    stage_h(0)
-    send_heads(2)
-    stage_f(1)
-    stage_c(3)
-    stage_e(2)
-    stage_d(3)
-    stage_h(1)
-    stage_f(2)
-    stage_e(3)
-    send_heads(3)
-    stage_h(2)
-    stage_f(3)
-    for copy in att_x:
-        copy.wait_recv()
-    att_cx = send(heads.at[tp_x], heads.at[tp_x], c_dev)
-    att_c.wait_recv()
-    att_cx.wait_recv()
-    stage_h(3)
-
     def project(i, carry):
         span = pl.ds(pl.multiple_of(i * piece, piece), piece)
         joined = jnp.concatenate([heads[t, span] for t in range(4)], axis=1)
@@ -398,7 +360,44 @@
         )
         return carry
 
+    for copy in halo:
+        copy.wait_recv()
+    lax.fori_loop(0, 1, attend, 0)
+    att_c = send(heads.at[tp], heads.at[tp], c_dev)
+    stage_a(3)
+    send_heads(0)
+    send_heads(1)
+    for load in loads:
+        load.wait()
+    stage_d(0)
+    stage_c(1)
+    stage_b(2)
+    send_heads(2)
+    send_heads(3)
+    stage_e(0)
+    stage_d(1)
+    stage_c(2)
+    stage_b(3)
+    stage_e(1)
+    stage_f(0)
+    stage_d(2)
+    stage_c(3)
+    stage_e(2)
+    stage_f(1)
+    stage_h(0)
+    stage_d(3)
+    stage_e(3)
+    for copy in att_x:
+        copy.wait_recv()
+    att_cx = send(heads.at[tp_x], heads.at[tp_x], c_dev)
+    stage_f(2)
+    stage_h(1)
+    stage_f(3)
+    stage_h(2)
+    att_c.wait_recv()
+    att_cx.wait_recv()
     lax.fori_loop(0, 4, project, 0)
+    stage_h(3)
     for s in range(1, groups):
         held[s]["home"].wait_recv()
     out_ref[...] = lax.dot_general(

time: 69.1 us -> 73.4 us (1.062)
  Pallas kernels: 65.1 us -> 69.5 us
    pallas_call x1, Pallas kernels: 65.1 us -> 69.5 us  [fused(): pl.pallas_call(functools.partial(fused_kernel, groups), out_shape=(jax.Sh...]
where the time goes in v4:
time: 73.4 us; the launch traced here: 73.2 us
  Pallas kernels  69.5 us (95%)
  local copies, waits for them, and re-layouts  3.12 us (4%)
    pallas_call x1, Pallas kernels, fused(): pl.pallas_call(functools.partial(fused_kernel, groups), out_shape=(jax.Sh...  69.5 us
    unnamed x4, local copies, waits for them, and re-layouts  3.12 us

profile of v4, /device:TPU:0, one launch (start us, length us, event | category | flops | bytes accessed | tf_op | source)
XLA Modules:
  0.0 73.2 jit_solution(4809435574701065080)
XLA Ops:
  0.6 69.5 %shard_map.140 = (bf16[1024,512]{1,0:T(8,128)(2,1)}, bf16[128,2048]{1,0:T(8,128)(2,1)}) custom-call(f32[4]{0:T(128)} %sink_ref.1, bf16[1024,256]{1,0:T(8,128)(2,1)} %q_ref.1, bf16[64,1024]{1,0:T(8,128)(2,1)} %bitcast.8, bf16[64,1024]{1,0:T(8,128)(2,1)} %bitcast.9, f32[1,2048]{1,0:T(1,128)} %bitcast.12, bf16[4,2048]{1,0:T(4,128)(2,1)} %bitcast.11, ...), custom_call_target="tpu_custom_call" | custom-call | flops 20000000000 | bytes 20000000 | tf_op jit(solution)/shard_map/pallas_call | solution.py:436
  70.1 0.0 copy-start
  70.1 2.3 %copy.17 = bf16[1024,512]{1,0:T(8,128)(2,1)} copy(bf16[1024,512]{1,0:T(8,128)(2,1)} %get-tuple-element.4) | data formatting | bytes 2097152
  72.4 0.0 copy-done
  72.4 0.8 %copy.18 = bf16[128,2048]{1,0:T(8,128)(2,1)} copy(bf16[128,2048]{1,0:T(8,128)(2,1)S(1)} %copy-done) | data formatting | bytes 1048576
Async XLA Ops:
  70.1 2.3 %copy-start = (bf16[128,2048]{1,0:T(8,128)(2,1)S(1)}, bf16[128,2048]{1,0:T(8,128)(2,1)}, u32[]{:S(2)}) copy-start(bf16[128,2048]{1,0:T(8,128)(2,1)} %get-tuple-element.5) | copy-start | bytes 1572868
